TPU v7x, 256 devices: a whole 4x4x8 slice. The times are simulated.
256 devices in a mesh: sp: 64 (over z, y, core), tp: 4 (over x).
Axes of the slice: x: 4, y: 4, z: 8, core: 2. Of those that a mesh axis runs over, the one named last changes fastest.
Arguments:
- residual: bfloat16 [24576, 2048], P(('sp', 'tp')), may hold values from -6 to 6
- query_one: bfloat16 [24576, 512], P('sp', 'tp'), may hold values from -6 to 6
- key_one: bfloat16 [24576, 512], P('sp', 'tp'), may hold values from -6 to 6
- value_one: bfloat16 [24576, 1024], P('sp', 'tp'), may hold values from -6 to 6
- gate_one: bfloat16 [24576, 1024], P('sp', 'tp'), may hold values from -6 to 6
- decay_one: bfloat16 [2, 24576, 512], P(None, 'sp', 'tp'), may hold values from -12 to 12
- norm_one: float32 [128], replicated, may hold values from 0.1 to 1.9
- output_one: bfloat16 [1024, 2048], P('tp'), may hold values from -0.125 to 0.125
- query_two: bfloat16 [24576, 1024], P('sp', 'tp'), may hold values from -6 to 6
- key_two: bfloat16 [24576, 1024], P('sp', 'tp'), may hold values from -6 to 6
- value_two: bfloat16 [24576, 1024], P('sp', 'tp'), may hold values from -6 to 6
- gate_two: bfloat16 [24576, 1024], P('sp', 'tp'), may hold values from -6 to 6
- decay_two: bfloat16 [2, 24576, 1024], P(None, 'sp', 'tp'), may hold values from -12 to 12
- norm_two: float32 [128], replicated, may hold values from 0.1 to 1.9
- output_two: bfloat16 [1024, 2048], P('tp'), may hold values from -0.125 to 0.125
- norm_gain: float32 [2048], replicated, may hold values from 0.1 to 1.9
- expert_ids: int32 [24576, 2], P('sp'), may hold values from 0 to 63, as said below
- group_weight: float32 [24576], P('sp'), may hold values from 0.25 to 1
- pair_weight: float32 [24576, 2], P('sp'), may hold values from 0.05 to 1
- expert_gate: bfloat16 [64, 2048, 1024], P('sp', None, 'tp'), may hold values from -0.125 to 0.125
- expert_up: bfloat16 [64, 2048, 1024], P('sp', None, 'tp'), may hold values from -0.125 to 0.125
- expert_down: bfloat16 [64, 1024, 2048], P('sp', 'tp'), may hold values from -0.1875 to 0.1875
Outputs:
- layer_out: bfloat16 [24576, 2048], P(('sp', 'tp'))
Inputs may be any that keep to these rules, and one draw needn't show every extreme that they name: `expert_ids`: each row names two different experts of one group, the group of expert e being e // 16. In each aligned block of 96 rows no expert is named more than 4 times, and one expert, the same in every block, is named exactly 4 times in each block.
All inputs are finite; a program needn't handle non-finite values.
Results may differ from a plain program's by a relative error of at most 0.018.
Values may be sent and summed in bfloat16 or wider, within the bound.
A program may use at most 128 MiB of HBM per device.

v0:
```python
import jax
import jax.numpy as jnp
from jax import lax
from jax.experimental import pallas as pl
from jax.experimental.pallas import tpu as pltpu
from jax.sharding import Mesh
from jax.sharding import PartitionSpec as P

D = 2048
BLOCK = 64
NB = 6
KEYS = 384
SP = ("sp_0", "sp_1", "sp_2")
SP_TP = ("sp_0", "sp_1", "sp_2", "tp")
EPS = 1e-06
F32 = jnp.float32
BF16 = jnp.bfloat16


def place():
    return tuple(lax.axis_index(a) for a in SP_TP)


def dev(z, y, c, x):
    return {"sp_0": z, "sp_1": y, "sp_2": c, "tp": x}


def remote(src, dst, ssem, rsem, device):
    return pltpu.make_async_remote_copy(
        src_ref=src,
        dst_ref=dst,
        send_sem=ssem,
        recv_sem=rsem,
        device_id=device,
        device_id_type=pl.DeviceIdType.MESH,
    )


def greet(barrier, device):
    pl.semaphore_signal(barrier, inc=1, device_id=device, device_id_type=pl.DeviceIdType.MESH)


def nn(a, b):
    return lax.dot_general(a, b, (((1,), (0,)), ((), ())), preferred_element_type=F32)


def nt(a, b):
    return lax.dot_general(a, b, (((1,), (1,)), ((), ())), preferred_element_type=F32)


def tn(a, b):
    return lax.dot_general(a, b, (((0,), (0,)), ((), ())), preferred_element_type=F32)


def iota2(shape, dim):
    return lax.broadcasted_iota(jnp.int32, shape, dim)


def halves(row):
    hi = row.astype(BF16)
    lo = (row - hi.astype(F32)).astype(BF16)
    return hi, lo


ORDER = (4, 0, 3, 5, 2, 6, 1, 7)
MIRROR = tuple(ORDER.index((-dz) % 8) for dz in ORDER)
CHUNKS = 4

INPUTS = (
    "res", "q1", "k1", "v1", "g1", "d1", "n1", "ow1", "q2", "k2", "v2", "g2", "d2", "n2", "ow2",
    "ng", "ids", "gw", "pw", "eg", "eu", "ed",
)


def dma(*n):
    return pltpu.SemaphoreType.DMA(n)


def scratch_shapes():
    vm = pltpu.VMEM
    slab = vm((64, 4, D), BF16)
    return {
        "q": vm((384, KEYS), BF16), "k": vm((384, KEYS), BF16), "v": vm((384, 512), BF16),
        "g": vm((384, 512), BF16), "d": vm((2, 384, KEYS), BF16), "gain": vm((1, 256), F32),
        "ngv": vm((1, D), F32), "idv": vm((2, 384), jnp.int32), "gwv": vm((384,), F32),
        "pwv": vm((2, 384), F32), "resv": vm((96, D), BF16), "ow": vm((512, D), BF16),
        "cum": vm((2, 384, KEYS), F32), "qd": vm((2, 384, KEYS), BF16), "kd": vm((2, 384, KEYS), BF16),
        "add": vm((2, NB, 128, KEYS), F32), "dec": vm((2, NB, 8, KEYS), F32),
        "acc": vm((384, 512), F32), "gs": vm((384, 512), F32), "st": vm((2, NB, 128, KEYS), BF16),
        "s1": vm((8, 40, KEYS), BF16), "r1": vm((8, 40, KEYS), BF16),
        "pre": vm((2, 8, 16, KEYS), F32), "prd": vm((2, 8, 8, KEYS), F32),
        "s2": vm((2, 24, KEYS), BF16), "r2": vm((8, 24, KEYS), BF16),
        "s3": vm((8, 32, KEYS), BF16), "r3": vm((8, 32, KEYS), BF16),
        "mixed": vm((384, 512), BF16), "pbuf": vm((4, 96, D), BF16), "prec": vm((4, 96, D), BF16),
        "stream": vm((96, D), BF16), "normed": vm((96, D), BF16),
        "sel": vm((256, 96), BF16), "whi": vm((256, 96), BF16), "wlo": vm((256, 96), BF16),
        "wg": vm((2, D, 256), BF16), "wu": vm((2, D, 256), BF16), "wd": vm((2, 256, D), BF16),
        "send": slab, "recv": slab, "ret": slab, "bk": slab,
        "xb": vm((512, D), BF16), "hid": vm((128, 512), BF16), "yown": vm((256, D), F32),
        "ypart": vm((256, D), BF16), "yrecv": vm((256, D), BF16), "bb": vm((256, D), BF16),
        "lsem": dma(25), "wsend": dma(3), "wrecv": dma(3), "xsem": dma(3), "rsem": dma(3),
        "dsend": dma(4), "drecv": dma(4), "ssem": dma(1), "srecv": dma(CHUNKS),
        "fsend": dma(CHUNKS), "frecv": dma(CHUNKS), "psend": dma(CHUNKS), "precv": dma(CHUNKS),
        "bsend": dma(1), "brecv": dma(CHUNKS),
    }


class Refs:
    def __init__(self, names, refs):
        self.__dict__.update(zip(names, refs))


def layer_kernel(*refs):
    shapes = scratch_shapes()
    r = Refs(INPUTS + ("out",) + tuple(shapes), refs)
    z, y, c, x = place()
    p = y * 2 + c
    sgn = (1 - 2 * (x % 2)) * (1 - 2 * c)
    friend = dev(z, y, c, (x + sgn + 4) % 4)
    facing = dev(z, y, c, (x - sgn + 4) % 4)

    def rank(dz, t):
        return dev((z + dz) % 8, t // 2, t % 2, x)

    plan = {
        "d": [(r.d1, r.d.at[:, :, 0:128]), (r.d2, r.d.at[:, :, 128:384])],
        "k": [(r.k1, r.k.at[:, 0:128]), (r.k2, r.k.at[:, 128:384])],
        "v": [(r.v1, r.v.at[:, 0:256]), (r.v2, r.v.at[:, 256:512])],
        "q": [(r.q1, r.q.at[:, 0:128]), (r.q2, r.q.at[:, 128:384])],
        "g": [(r.g1, r.g.at[:, 0:256]), (r.g2, r.g.at[:, 256:512]),
              (r.n1, r.gain.at[:, 0:128]), (r.n2, r.gain.at[:, 128:256])],
        "i": [(r.ids, r.idv), (r.gw, r.gwv), (r.pw, r.pwv)],
        "o": [(r.ow1, r.ow.at[pl.ds(0, 256)]), (r.ow2, r.ow.at[pl.ds(256, 256)])],
        "s": [(r.res, r.resv), (r.ng, r.ngv)],
        "w": [(r.eg.at[0], r.wg.at[0]), (r.eu.at[0], r.wu.at[0]), (r.ed.at[0], r.wd.at[0])],
    }
    loads, count = {}, 0
    for name, pairs in plan.items():
        loads[name] = []
        for src, dst in pairs:
            cp = pltpu.make_async_copy(src, dst, r.lsem.at[count])
            count += 1
            cp.start()
            loads[name].append(cp)

    def loaded(names):
        for name in names:
            for cp in loads[name]:
                cp.wait()

    barrier = pltpu.get_barrier_semaphore()

    @pl.loop(1, 64)
    def _(o):
        t = (z * 8 + p + o) % 64
        greet(barrier, dev(t // 8, (t // 2) % 4, t % 2, x))

    for o in range(1, 4):
        greet(barrier, dev(z, y, c, (x + o) % 4))

    row = iota2((BLOCK, BLOCK), 0)
    col = iota2((BLOCK, BLOCK), 1)
    lower, upper = row >= col, row <= col
    tri = tuple(jnp.where(m, 1.0, 0.0).astype(BF16) for m in (lower, upper))
    tri = tuple(jnp.concatenate([t, t, t], axis=1) for t in tri)
    scale = jnp.where(iota2((1, KEYS), 1) < 128, 64.0 ** -0.5, 128.0 ** -0.5)
    lane = iota2((1, 256), 1) % 128 < 64
    zero = jnp.zeros((), BF16)
    SPANS = (slice(0, 128), slice(0, 128), slice(128, 256), slice(256, 384))

    def keys_of(n):
        rows = pl.ds(n * BLOCK, BLOCK)
        k = r.k[rows, :].astype(F32)
        ends = []
        for way in range(2):
            d = r.d[way, rows, :].astype(F32)
            rate = (jnp.minimum(d, 0.0) - jnp.log1p(jnp.exp(-jnp.abs(d)))) * (1.0 / 16.0)
            hi = rate.astype(BF16)
            rest = rate - hi.astype(F32)
            mid = rest.astype(BF16)
            low = (rest - mid.astype(F32)).astype(BF16)
            cum = nn(tri[way], jnp.concatenate([hi, mid, low], axis=0))
            r.cum[way, rows, :] = cum
            fade = jnp.exp(cum[BLOCK - 1 :, :] if way == 0 else cum[0:1, :])
            kd = k * jnp.exp(-cum)
            r.kd[way, rows, :] = kd.astype(BF16)
            r.dec[way, n] = jnp.broadcast_to(fade, (8, KEYS))
            ends.append((kd * fade).astype(BF16))
        both = []
        for h, at in enumerate(SPANS):
            v = r.v[rows, 128 * h : 128 * h + 128]
            both.append(tn(v, jnp.concatenate([ends[0][:, at], ends[1][:, at]], axis=1)))
        both[0:2] = [jnp.where(lane, both[0], both[1])]
        for way in range(2):
            for i, b in enumerate(both):
                r.add[way, n, :, 128 * i : 128 * i + 128] = b[:, 128 * way : 128 * way + 128]

    loaded("dkv")
    for n in range(NB):
        keys_of(n)

    pl.semaphore_wait(barrier, 66)
    weights = [
        remote(src.at[0], dst.at[1], r.wsend.at[i], r.wrecv.at[i], friend)
        for i, (src, dst) in enumerate(((r.eg, r.wg), (r.eu, r.wu), (r.ed, r.wd)))
    ]
    weights[0].start()
    weights[1].start()

    totals, fades = [], []
    for way in range(2):
        order = range(NB) if way == 0 else range(NB - 1, -1, -1)
        run, fade = None, None
        for n in order:
            f = r.dec[way, n][0:1]
            run = r.add[way, n] if run is None else run * f + r.add[way, n]
            fade = f if fade is None else fade * f
        totals.append(run.astype(BF16))
        fades.append(fade)
    tile = jnp.concatenate([t.astype(F32) for f in fades for t in halves(f)] * 2, axis=0).astype(BF16)
    for j in range(8):
        r.s1[j, 0:16, :] = totals[0][16 * j : 16 * j + 16]
        r.s1[j, 16:32, :] = totals[1][16 * j : 16 * j + 16]
        r.s1[j, 32:40, :] = tile
    r.r1[p] = r.s1[p]

    def plane_copy(src, dst, i, o):
        t = (p + o) % 8
        return remote(src.at[t], dst.at[p], r.xsem.at[i], r.rsem.at[i], rank(0, t))

    for o in (4, 3, 5, 2, 6, 1, 7):
        plane_copy(r.s1, r.r1, 0, o).start()

    def queries_of(n):
        rows = pl.ds(n * BLOCK, BLOCK)
        q = r.q[rows, :].astype(F32) * scale
        for way in range(2):
            r.qd[way, rows, :] = (q * jnp.exp(r.cum[way, rows, :])).astype(BF16)

    def inner(n):
        rows = pl.ds(n * BLOCK, BLOCK)
        for h, at in enumerate(SPANS):
            m = None if h > 1 else lane[:, 0:128] if h == 0 else jnp.logical_not(lane[:, 0:128])
            s = []
            for way in range(2):
                qd = r.qd[way, rows, at]
                s.append(nt(qd if m is None else jnp.where(m, qd, zero), r.kd[way, rows, at]))
            s = jnp.where(lower, s[0], 0.0) + jnp.where(upper, s[1], 0.0)
            head = slice(128 * h, 128 * h + 128)
            r.acc[rows, head] = nn(s.astype(BF16), r.v[rows, head])

    loaded("q")
    for n in range(NB):
        queries_of(n)
    for n in range(3):
        inner(n)

    def seven(src, dst, i):
        return remote(src.at[pl.ds(0, 7)], dst.at[pl.ds(0, 7)], r.xsem.at[i], r.rsem.at[i], facing)

    batches = [seven(r.s1, r.r1, 0), seven(r.r2, r.r2, 1), seven(r.s3, r.r3, 2)]
    batches[0].wait_recv()

    def unpack(i):
        s = r.r1[i].astype(F32)
        return s[0:16], s[16:32], s[32:33] + s[33:34], s[34:35] + s[35:36]

    parts = [unpack(i) for i in range(8)]
    for way in range(2):
        run, fade = jnp.zeros((16, KEYS), F32), jnp.ones((1, KEYS), F32)
        for i in range(8) if way == 0 else range(7, -1, -1):
            r.pre[way, i] = run
            r.prd[way, i] = jnp.broadcast_to(fade, (8, KEYS))
            run = run * parts[i][2 + way] + parts[i][way]
            fade = fade * parts[i][2 + way]
        hi, lo = halves(fade)
        r.s2[way, 0:16, :] = run.astype(BF16)
        r.s2[way, 16:24, :] = jnp.concatenate([hi.astype(F32), lo.astype(F32)] * 4, axis=0).astype(BF16)
    r.r2[z] = r.s2[0]
    for o in (4, 3, 5, 2, 6, 1, 7):
        remote(r.s2.at[(z + o) // 8], r.r2.at[z], r.xsem.at[1], r.rsem.at[1], rank(o, p)).start()

    for n in range(3, NB):
        inner(n)

    loaded("i")

    def mine(ref):
        pick = ref[:, 288:384]
        for i in (2, 1, 0):
            pick = jnp.where(x == i, ref[:, 96 * i : 96 * i + 96], pick)
        return pick

    ids, gate, pair = mine(r.idv), mine(r.gwv[...][None]), mine(r.pwv)
    inv = gate / (pair[0:1] + pair[1:2])
    experts = iota2((64, 96), 0)
    named = [jnp.where(ids[k : k + 1] == experts, 1.0, 0.0) for k in range(2)]
    before = jnp.where(iota2((96, 96), 0) < iota2((96, 96), 1), 1.0, 0.0).astype(BF16)
    count = nn((named[0] + named[1]).astype(BF16), before)
    slots = [
        jnp.sum(count * named[k], axis=0, keepdims=True).astype(jnp.int32) + 4 * ids[k : k + 1] for k in range(2)
    ]
    for i, dz in enumerate(ORDER):
        here = iota2((32, 96), 0) + 32 * ((z + dz) % 8)
        hits = [jnp.where(slots[k] == here, 1.0, 0.0) for k in range(2)]
        at = slice(32 * i, 32 * i + 32)
        r.sel[at, :] = (hits[0] + hits[1]).astype(BF16)
        r.whi[at, :], r.wlo[at, :] = halves(hits[0] * (inv * pair[0:1]) + hits[1] * (inv * pair[1:2]))

    batches[1].wait_recv()
    entry = []
    for way in range(2):
        run = jnp.zeros((16, KEYS), F32)
        for i in range(8) if way == 0 else range(7, -1, -1):
            s = r.r2[i].astype(F32)
            run = jnp.where(i < z if way == 0 else i > z, run * (s[16:17] + s[17:18]) + s[0:16], run)
        entry.append(run)
    for j in range(8):
        for way in range(2):
            r.s3[j, 16 * way : 16 * way + 16, :] = (
                r.pre[way, j] + r.prd[way, j][0:1] * entry[way]
            ).astype(BF16)
    r.r3[p] = r.s3[p]
    for o in (4, 3, 5, 2, 6, 1, 7):
        plane_copy(r.s3, r.r3, 2, o).start()

    loaded("g")
    for n in range(NB):
        rows = pl.ds(n * BLOCK, BLOCK)
        g = r.g[rows, :].astype(F32)
        gain = r.gain[...]
        gain = jnp.concatenate([gain[:, 0:128], gain[:, 0:128], gain[:, 128:256], gain[:, 128:256]], axis=1)
        r.gs[rows, :] = gain * (g / (1.0 + jnp.exp(-g)))

    batches[2].wait_recv()
    for way in range(2):
        state = jnp.concatenate([r.r3[j, 16 * way : 16 * way + 16, :] for j in range(8)], axis=0).astype(F32)
        for n in range(NB) if way == 0 else range(NB - 1, -1, -1):
            r.st[way, n] = state.astype(BF16)
            state = state * r.dec[way, n][0:1] + r.add[way, n]

    def read_out(n):
        rows = pl.ds(pl.multiple_of(n * BLOCK, BLOCK), BLOCK)
        for h, at in enumerate(SPANS):
            qd = jnp.concatenate([r.qd[0, rows, at], r.qd[1, rows, at]], axis=1)
            if h < 2:
                qd = jnp.where(lane if h == 0 else jnp.logical_not(lane), qd, zero)
            head = slice(128 * h, 128 * h + 128)
            t = r.acc[rows, head] + nt(qd, jnp.concatenate([r.st[0, n, :, at], r.st[1, n, :, at]], axis=1))
            t = t * lax.rsqrt(jnp.mean(t * t, axis=1, keepdims=True) + EPS)
            r.mixed[rows, head] = (t * r.gs[rows, head]).astype(BF16)

    def to_owner(o):
        return remote(r.pbuf.at[o], r.prec.at[o], r.dsend.at[o], r.drecv.at[o], dev(z, y, c, (x + o) % 4))

    def project(t, away):
        o = (t - x + 4) % 4
        rows = r.mixed[pl.ds(pl.multiple_of(t * 96, 32), 96), :]
        for q in range(4):
            at = slice(512 * q, 512 * q + 512)
            r.pbuf[o, :, at] = nn(rows, r.ow[:, at]).astype(BF16)
        if away:
            to_owner(o).start()

    across = (x + 2) % 4
    half = across // 2
    for i in range(3):
        read_out(3 * half + i)
    loaded("o")
    project(across, True)
    project(across + 1 - 2 * (across % 2), True)
    for i in range(3):
        read_out(3 * (1 - half) + i)
    project(x + 1 - 2 * (x % 2), True)
    weights[2].start()
    project(x, False)

    loaded("s")
    for o in (1, 3, 2):
        to_owner(o).wait_recv()
    for q in range(4):
        at = slice(512 * q, 512 * q + 512)
        total = r.pbuf[0, :, at].astype(F32)
        for o in (1, 3, 2):
            total = total + r.prec[o, :, at].astype(F32)
        r.stream[:, at] = (r.resv[:, at].astype(F32) + total.astype(BF16).astype(F32)).astype(BF16)
    wide = r.stream[...].astype(F32)
    ms = jnp.mean(wide * wide, axis=1, keepdims=True)
    r.normed[...] = (wide * lax.rsqrt(ms + EPS) * r.ngv[...]).astype(BF16)

    def scatter_rows(dst, first, rows, at):
        for e in range(rows.shape[0] // 4):
            dst[first + e, :, at] = rows[4 * e : 4 * e + 4, :]

    def slabs_out(src, dst, ssem, rsem, k):
        for i in (2 * k, 2 * k + 1):
            @pl.loop(1 if ORDER[i] == 0 else 0, 8)
            def _(o):
                t = (p + o) % 8
                remote(
                    src.at[i * 8 + t], dst.at[MIRROR[i] * 8 + p], ssem.at[0], rsem.at[k], rank(ORDER[i], t)
                ).start()

    def slabs_in(src, dst, ssem, rsem, k):
        n = 15 if k == 0 else 16
        return remote(src.at[pl.ds(0, n)], dst.at[pl.ds(0, n)], ssem.at[0], rsem.at[k], facing)

    for k in range(CHUNKS):
        for q in range(4):
            at = slice(512 * q, 512 * q + 512)
            rows = nn(r.sel[64 * k : 64 * k + 64, :], r.normed[:, at])
            scatter_rows(r.send, 16 * k, rows.astype(BF16), at)
        if k == 0:
            r.recv[8 + p] = r.send[8 + p]
        slabs_out(r.send, r.recv, r.ssem, r.srecv, k)

    def forward(k):
        return remote(
            r.xb.at[pl.ds(128 * k, 64)], r.xb.at[pl.ds(128 * k + 64, 64)], r.fsend.at[k], r.frecv.at[k], facing
        )

    def partial(k):
        span = pl.ds(64 * k, 64)
        return remote(r.ypart.at[span], r.yrecv.at[span], r.psend.at[k], r.precv.at[k], facing)

    def arrive(k):
        slabs_in(r.send, r.recv, r.ssem, r.srecv, k).wait_recv()
        for i in range(2):
            r.xb[128 * k + 32 * i : 128 * k + 32 * i + 32, :] = jnp.concatenate(
                [r.recv[16 * k + 8 * i + j] for j in range(8)], axis=0
            )
        forward(k).start()

    def experts_on(k):
        if k == 0:
            loaded("w")
            weights[0].wait_recv()
            weights[1].wait_recv()
        forward(k).wait_recv()
        rows = pl.ds(128 * k, 128)
        for s in range(2):
            a = nn(r.xb[rows, :], r.wg[s])
            b = nn(r.xb[rows, :], r.wu[s])
            r.hid[:, 256 * s : 256 * s + 256] = (a / (1.0 + jnp.exp(-a)) * b).astype(BF16)
        if k == 0:
            weights[2].wait_recv()
        for q in range(4):
            at = slice(512 * q, 512 * q + 512)
            out = nn(r.hid[:, 0:256], r.wd[0, :, at]) + nn(r.hid[:, 256:512], r.wd[1, :, at])
            r.yown[64 * k : 64 * k + 64, at] = out[0:64]
            r.ypart[64 * k : 64 * k + 64, at] = out[64:128].astype(BF16)
        partial(k).start()

    def give_back(k):
        partial(k).wait_recv()
        span = slice(64 * k, 64 * k + 64)
        for q in range(4):
            at = slice(512 * q, 512 * q + 512)
            rows = r.yown[span, at] + r.yrecv[span, at].astype(F32)
            scatter_rows(r.ret, 16 * k, rows.astype(BF16), at)
        if k == 0:
            r.bk[8 + p] = r.ret[8 + p]
        slabs_out(r.ret, r.bk, r.bsend, r.brecv, k)

    arrive(0)
    experts_on(0)
    arrive(1)
    experts_on(1)
    give_back(0)
    arrive(2)
    arrive(3)
    give_back(1)
    experts_on(2)
    experts_on(3)
    give_back(2)
    give_back(3)

    def gather_back(k):
        slabs_in(r.ret, r.bk, r.bsend, r.brecv, k).wait_recv()
        for i in range(2):
            r.bb[64 * k + 32 * i : 64 * k + 32 * i + 32, :] = jnp.concatenate(
                [r.bk[16 * k + 8 * i + j] for j in range(8)], axis=0
            )

    def combined(first, last, at):
        return tn(r.whi[first:last, :], r.bb[first:last, at]) + tn(r.wlo[first:last, :], r.bb[first:last, at])

    for k in range(3):
        gather_back(k)
    early = [combined(0, 192, slice(512 * q, 512 * q + 512)) for q in range(4)]
    gather_back(3)
    for q in range(4):
        at = slice(512 * q, 512 * q + 512)
        total = r.stream[:, at].astype(F32) + early[q] + combined(192, 256, at)
        r.out[:, at] = total.astype(BF16)

    for batch in batches:
        batch.wait_send()
    for o in (1, 2, 3):
        to_owner(o).wait_send()
    for cp in weights:
        cp.wait_send()
    for src, dst, ssem, rsem in ((r.send, r.recv, r.ssem, r.srecv), (r.ret, r.bk, r.bsend, r.brecv)):
        remote(src.at[pl.ds(0, 63)], dst.at[pl.ds(0, 63)], ssem.at[0], rsem.at[0], facing).wait_send()
    for k in range(CHUNKS):
        forward(k).wait_send()
        partial(k).wait_send()


def body(
    residual, query_one, key_one, value_one, gate_one, decay_one, norm_one, output_one,
    query_two, key_two, value_two, gate_two, decay_two, norm_two, output_two, norm_gain,
    expert_ids, group_weight, pair_weight, expert_gate, expert_up, expert_down,
):
    return pl.pallas_call(
        layer_kernel,
        name="layer",
        out_shape=jax.ShapeDtypeStruct((96, D), BF16),
        in_specs=[pl.BlockSpec(memory_space=pltpu.HBM)] * len(INPUTS),
        out_specs=pl.BlockSpec(memory_space=pltpu.VMEM),
        scratch_shapes=list(scratch_shapes().values()),
        compiler_params=pltpu.CompilerParams(
            collective_id=0, has_side_effects=True, vmem_limit_bytes=60 * 1024 * 1024
        ),
    )(
        residual, query_one, key_one, value_one, gate_one, decay_one, norm_one[None], output_one,
        query_two, key_two, value_two, gate_two, decay_two, norm_two[None], output_two, norm_gain[None],
        expert_ids.T, group_weight, pair_weight.T, expert_gate, expert_up, expert_down,
    )


def solution(mesh):
    torus = Mesh(mesh.devices.reshape(8, 4, 2, mesh.shape["tp"]), SP_TP)
    heads = P(SP, "tp")
    in_specs = (
        P(SP_TP, None), heads, heads, heads, heads, P(None, SP, "tp"), P(), P("tp", None),
        heads, heads, heads, heads, P(None, SP, "tp"), P(), P("tp", None),
        P(), P(SP, None), P(SP), P(SP, None), P(SP, None, "tp"), P(SP, None, "tp"), P(SP, "tp", None),
    )
    return jax.shard_map(body, mesh=torus, in_specs=in_specs, out_specs=P(SP_TP, None), check_vma=False)
```

profile of v0, /device:TPU:1, one launch (start us, length us, event | category | flops | bytes accessed | tf_op | source)
XLA Modules:
  0.0 112.1 jit_solution(17762638369728617009)
XLA Ops:
  0.0 110.3 %layer.1 = bf16[96,2048]{1,0:T(8,128)(2,1)} custom-call(bf16[96,2048]{1,0:T(8,128)(2,1)} %refs_0_.1, bf16[384,128]{1,0:T(8,128)(2,1)} %refs_1_.1, bf16[384,128]{1,0:T(8,128)(2,1)} %refs_2_.1, bf16[384,256]{1,0:T(8,128)(2,1)} %refs_3_.1, bf16[384,256]{1,0:T(8,128)(2,1)} %refs_4_.1, bf16[2,384,128]{2,1,0:T(8,128)(2,1)} %refs_5_.1, f32[1,128]{1,0:T(1,128)} %bitcast.8, ...), custom_call_target="tpu_custom_call" | custom-call | tf_op jit(solution)/shard_map/layer/pallas_call | solution.py:515
  110.3 1.8 %copy.24 = bf16[96,2048]{1,0:T(8,128)(2,1)} copy(bf16[96,2048]{1,0:T(8,128)(2,1)} %layer.1) | data formatting | bytes 786432
where the time goes:
time: 112 us
  Pallas kernels  110 us (98%)
  local copies, waits for them, and re-layouts  1.77 us (2%)
    pallas_call x1, Pallas kernels, body(): pl.pallas_call(layer_kernel, name='layer', out_shape=jax.ShapeDtypeStruct...  110 us

commit v1 on v0

--- a/solution.py
+++ b/solution.py
@@ -65,6 +65,7 @@
 ORDER = (4, 0, 3, 5, 2, 6, 1, 7)
 MIRROR = tuple(ORDER.index((-dz) % 8) for dz in ORDER)
 CHUNKS = 4
+HALF = D // 2
 
 INPUTS = (
     "res", "q1", "k1", "v1", "g1", "d1", "n1", "ow1", "q2", "k2", "v2", "g2", "d2", "n2", "ow2",
@@ -91,15 +92,16 @@
         "pre": vm((2, 8, 16, KEYS), F32), "prd": vm((2, 8, 8, KEYS), F32),
         "s2": vm((2, 24, KEYS), BF16), "r2": vm((8, 24, KEYS), BF16),
         "s3": vm((8, 32, KEYS), BF16), "r3": vm((8, 32, KEYS), BF16),
-        "mixed": vm((384, 512), BF16), "pbuf": vm((4, 96, D), BF16), "prec": vm((4, 96, D), BF16),
-        "stream": vm((96, D), BF16), "normed": vm((96, D), BF16),
+        "mixed": vm((384, 512), BF16), "pbuf": vm((2, 4, 96, HALF), BF16), "prec": vm((2, 2, 96, HALF), BF16), "hop": vm((2, 2, 48, HALF), BF16),
+        "stream": vm((96, D), BF16), "oacc": vm((96, D), F32),
         "sel": vm((256, 96), BF16), "whi": vm((256, 96), BF16), "wlo": vm((256, 96), BF16),
         "wg": vm((2, D, 256), BF16), "wu": vm((2, D, 256), BF16), "wd": vm((2, 256, D), BF16),
-        "send": slab, "recv": slab, "ret": slab, "bk": slab,
+        "send0": vm((64, 4, HALF), BF16), "recv0": vm((64, 4, HALF), BF16),
+        "send1": vm((64, 4, HALF + 128), BF16), "recv1": vm((64, 4, HALF + 128), BF16), "ret": slab, "bk": slab,
         "xb": vm((512, D), BF16), "hid": vm((128, 512), BF16), "yown": vm((256, D), F32),
         "ypart": vm((256, D), BF16), "yrecv": vm((256, D), BF16), "bb": vm((256, D), BF16),
-        "lsem": dma(25), "wsend": dma(3), "wrecv": dma(3), "xsem": dma(3), "rsem": dma(3),
-        "dsend": dma(4), "drecv": dma(4), "ssem": dma(1), "srecv": dma(CHUNKS),
+        "lsem": dma(25), "wsend": dma(4), "wrecv": dma(4), "xsem": dma(3), "rsem": dma(3),
+        "dsend": dma(8), "drecv": dma(8), "hsend": dma(4), "hrecv": dma(4), "ssem": dma(2), "srecv": dma(2 * CHUNKS),
         "fsend": dma(CHUNKS), "frecv": dma(CHUNKS), "psend": dma(CHUNKS), "precv": dma(CHUNKS),
         "bsend": dma(1), "brecv": dma(CHUNKS),
     }
@@ -201,8 +203,13 @@
 
     pl.semaphore_wait(barrier, 66)
     weights = [
-        remote(src.at[0], dst.at[1], r.wsend.at[i], r.wrecv.at[i], friend)
-        for i, (src, dst) in enumerate(((r.eg, r.wg), (r.eu, r.wu), (r.ed, r.wd)))
+        remote(src, dst, r.wsend.at[i], r.wrecv.at[i], friend)
+        for i, (src, dst) in enumerate((
+            (r.eg.at[0], r.wg.at[1]),
+            (r.eu.at[0, pl.ds(0, HALF)], r.wu.at[1, pl.ds(0, HALF)]),
+            (r.eu.at[0, pl.ds(HALF, HALF)], r.wu.at[1, pl.ds(HALF, HALF)]),
+            (r.ed.at[0], r.wd.at[1]),
+        ))
     ]
     weights[0].start()
     weights[1].start()
@@ -350,43 +357,80 @@
             t = t * lax.rsqrt(jnp.mean(t * t, axis=1, keepdims=True) + EPS)
             r.mixed[rows, head] = (t * r.gs[rows, head]).astype(BF16)
 
-    def to_owner(o):
-        return remote(r.pbuf.at[o], r.prec.at[o], r.dsend.at[o], r.drecv.at[o], dev(z, y, c, (x + o) % 4))
-
-    def project(t, away):
-        o = (t - x + 4) % 4
+    def beside(side):
+        return dev(z, y, c, (x + 1 + 2 * side) % 4)
+
+    def band(i):
+        return pl.ds(pl.multiple_of(48 * i, 16), 48)
+
+    def hop_copy(cs, side):
+        i = 2 * cs + side
+        return remote(r.pbuf.at[cs, 3, band(side)], r.hop.at[cs, side], r.hsend.at[i], r.hrecv.at[i], beside(side))
+
+    def owner_copy(cs, side, merged):
+        rows = band(side if merged else 1 - side)
+        i = 4 * cs + 2 * side + (1 if merged else 0)
+        return remote(r.pbuf.at[cs, 1 + side, rows], r.prec.at[cs, side, rows], r.dsend.at[i], r.drecv.at[i], beside(side))
+
+    def project(t, slot, cs):
         rows = r.mixed[pl.ds(pl.multiple_of(t * 96, 32), 96), :]
-        for q in range(4):
+        for q in range(2):
             at = slice(512 * q, 512 * q + 512)
-            r.pbuf[o, :, at] = nn(rows, r.ow[:, at]).astype(BF16)
-        if away:
-            to_owner(o).start()
+            r.pbuf[cs, slot, :, at] = nn(rows, r.ow[:, HALF * cs + 512 * q : HALF * cs + 512 * q + 512]).astype(BF16)
+
+    def to_neighbour(side, cs):
+        project((x + 1 + 2 * side) % 4, 1 + side, cs)
+        owner_copy(cs, side, False).start()
+
+    def merge(cs, side):
+        hop_copy(cs, side).wait_recv()
+        rows = band(side)
+        for q in range(2):
+            at = slice(512 * q, 512 * q + 512)
+            both = r.pbuf[cs, 1 + side, rows, at].astype(F32) + r.hop[cs, side, :, at].astype(F32)
+            r.pbuf[cs, 1 + side, rows, at] = both.astype(BF16)
+        owner_copy(cs, side, True).start()
+
+    def own_rows(cs):
+        for side in range(2):
+            for merged in (False, True):
+                owner_copy(cs, side, merged).wait_recv()
+        for q in range(2):
+            at = slice(512 * q, 512 * q + 512)
+            wide = slice(HALF * cs + 512 * q, HALF * cs + 512 * q + 512)
+            total = r.pbuf[cs, 0, :, at].astype(F32)
+            for side in range(2):
+                total = total + r.prec[cs, side, :, at].astype(F32)
+            r.stream[:, wide] = (r.resv[:, wide].astype(F32) + total.astype(BF16).astype(F32)).astype(BF16)
 
     across = (x + 2) % 4
     half = across // 2
+    near = 1 - x % 2
+    far = 1 - near
     for i in range(3):
         read_out(3 * half + i)
     loaded("o")
-    project(across, True)
-    project(across + 1 - 2 * (across % 2), True)
+    project(across, 3, 0)
+    hop_copy(0, 0).start()
+    hop_copy(0, 1).start()
     for i in range(3):
         read_out(3 * (1 - half) + i)
-    project(x + 1 - 2 * (x % 2), True)
+    to_neighbour(near, 0)
+    to_neighbour(far, 0)
+    project(across, 3, 1)
+    hop_copy(1, 0).start()
+    hop_copy(1, 1).start()
+    merge(0, near)
+    merge(0, far)
+    to_neighbour(near, 1)
+    to_neighbour(far, 1)
+    project(x, 0, 0)
+    project(x, 0, 1)
+    merge(1, near)
+    merge(1, far)
     weights[2].start()
-    project(x, False)
-
+    weights[3].start()
     loaded("s")
-    for o in (1, 3, 2):
-        to_owner(o).wait_recv()
-    for q in range(4):
-        at = slice(512 * q, 512 * q + 512)
-        total = r.pbuf[0, :, at].astype(F32)
-        for o in (1, 3, 2):
-            total = total + r.prec[o, :, at].astype(F32)
-        r.stream[:, at] = (r.resv[:, at].astype(F32) + total.astype(BF16).astype(F32)).astype(BF16)
-    wide = r.stream[...].astype(F32)
-    ms = jnp.mean(wide * wide, axis=1, keepdims=True)
-    r.normed[...] = (wide * lax.rsqrt(ms + EPS) * r.ngv[...]).astype(BF16)
 
     def scatter_rows(dst, first, rows, at):
         for e in range(rows.shape[0] // 4):
@@ -397,22 +441,54 @@
             @pl.loop(1 if ORDER[i] == 0 else 0, 8)
             def _(o):
                 t = (p + o) % 8
-                remote(
-                    src.at[i * 8 + t], dst.at[MIRROR[i] * 8 + p], ssem.at[0], rsem.at[k], rank(ORDER[i], t)
-                ).start()
+                remote(src.at[i * 8 + t], dst.at[MIRROR[i] * 8 + p], ssem, rsem, rank(ORDER[i], t)).start()
 
     def slabs_in(src, dst, ssem, rsem, k):
         n = 15 if k == 0 else 16
-        return remote(src.at[pl.ds(0, n)], dst.at[pl.ds(0, n)], ssem.at[0], rsem.at[k], facing)
-
-    for k in range(CHUNKS):
-        for q in range(4):
+        return remote(src.at[pl.ds(0, n)], dst.at[pl.ds(0, n)], ssem, rsem, facing)
+
+    sides = ((r.send0, r.recv0), (r.send1, r.recv1))
+
+    def fill(cs, k):
+        span = slice(64 * k, 64 * k + 64)
+        for q in range(2):
             at = slice(512 * q, 512 * q + 512)
-            rows = nn(r.sel[64 * k : 64 * k + 64, :], r.normed[:, at])
-            scatter_rows(r.send, 16 * k, rows.astype(BF16), at)
+            rows = nn(r.sel[span, :], r.stream[:, HALF * cs + 512 * q : HALF * cs + 512 * q + 512])
+            scatter_rows(sides[cs][0], 16 * k, rows.astype(BF16), at)
+        if cs:
+            scatter_rows(r.send1, 16 * k, nn(r.sel[span, :], scales).astype(BF16), slice(HALF, HALF + 128))
         if k == 0:
-            r.recv[8 + p] = r.send[8 + p]
-        slabs_out(r.send, r.recv, r.ssem, r.srecv, k)
+            sides[cs][1][8 + p] = sides[cs][0][8 + p]
+
+    def dispatch(cs, k):
+        slabs_out(*sides[cs], r.ssem.at[cs], r.srecv.at[4 * cs + k], k)
+
+    own_rows(0)
+    fill(0, 0)
+    dispatch(0, 0)
+    fill(0, 1)
+    dispatch(0, 1)
+    fill(0, 2)
+    fill(0, 3)
+    own_rows(1)
+    wide = r.stream[...].astype(F32)
+    inv_rms = lax.rsqrt(jnp.mean(wide * wide, axis=1, keepdims=True) + EPS)
+    hi = inv_rms.astype(BF16).astype(F32)
+    mid = (inv_rms - hi).astype(BF16).astype(F32)
+    low = inv_rms - hi - mid
+    which = iota2((96, 128), 1)
+    scales = jnp.where(which == 0, hi, jnp.where(which == 1, mid, jnp.where(which == 2, low, 0.0))).astype(BF16)
+    fill(1, 0)
+    dispatch(1, 0)
+    fill(1, 1)
+    dispatch(1, 1)
+    dispatch(0, 2)
+    dispatch(0, 3)
+    fill(1, 2)
+    dispatch(1, 2)
+    fill(1, 3)
+    dispatch(1, 3)
+    r.oacc[...] = wide
 
     def forward(k):
         return remote(
@@ -424,18 +500,24 @@
         return remote(r.ypart.at[span], r.yrecv.at[span], r.psend.at[k], r.precv.at[k], facing)
 
     def arrive(k):
-        slabs_in(r.send, r.recv, r.ssem, r.srecv, k).wait_recv()
+        for cs in range(2):
+            slabs_in(*sides[cs], r.ssem.at[cs], r.srecv.at[4 * cs + k], k).wait_recv()
         for i in range(2):
-            r.xb[128 * k + 32 * i : 128 * k + 32 * i + 32, :] = jnp.concatenate(
-                [r.recv[16 * k + 8 * i + j] for j in range(8)], axis=0
+            rows = slice(128 * k + 32 * i, 128 * k + 32 * i + 32)
+            first, last = (
+                jnp.concatenate([ref[16 * k + 8 * i + j] for j in range(8)], axis=0).astype(F32)
+                for ref in (r.recv0, r.recv1)
             )
+            inv_rms = jnp.sum(last[:, HALF:], axis=1, keepdims=True)
+            r.xb[rows, 0:HALF] = (first * inv_rms * r.ngv[:, 0:HALF]).astype(BF16)
+            r.xb[rows, HALF:D] = (last[:, 0:HALF] * inv_rms * r.ngv[:, HALF:D]).astype(BF16)
         forward(k).start()
 
     def experts_on(k):
         if k == 0:
             loaded("w")
-            weights[0].wait_recv()
-            weights[1].wait_recv()
+            for cp in weights[0:3]:
+                cp.wait_recv()
         forward(k).wait_recv()
         rows = pl.ds(128 * k, 128)
         for s in range(2):
@@ -443,7 +525,7 @@
             b = nn(r.xb[rows, :], r.wu[s])
             r.hid[:, 256 * s : 256 * s + 256] = (a / (1.0 + jnp.exp(-a)) * b).astype(BF16)
         if k == 0:
-            weights[2].wait_recv()
+            weights[3].wait_recv()
         for q in range(4):
             at = slice(512 * q, 512 * q + 512)
             out = nn(r.hid[:, 0:256], r.wd[0, :, at]) + nn(r.hid[:, 256:512], r.wd[1, :, at])
@@ -460,11 +542,11 @@
             scatter_rows(r.ret, 16 * k, rows.astype(BF16), at)
         if k == 0:
             r.bk[8 + p] = r.ret[8 + p]
-        slabs_out(r.ret, r.bk, r.bsend, r.brecv, k)
+        slabs_out(r.ret, r.bk, r.bsend.at[0], r.brecv.at[k], k)
 
     arrive(0)
+    arrive(1)
     experts_on(0)
-    arrive(1)
     experts_on(1)
     give_back(0)
     arrive(2)
@@ -476,32 +558,38 @@
     give_back(3)
 
     def gather_back(k):
-        slabs_in(r.ret, r.bk, r.bsend, r.brecv, k).wait_recv()
+        slabs_in(r.ret, r.bk, r.bsend.at[0], r.brecv.at[k], k).wait_recv()
         for i in range(2):
             r.bb[64 * k + 32 * i : 64 * k + 32 * i + 32, :] = jnp.concatenate(
                 [r.bk[16 * k + 8 * i + j] for j in range(8)], axis=0
             )
 
-    def combined(first, last, at):
-        return tn(r.whi[first:last, :], r.bb[first:last, at]) + tn(r.wlo[first:last, :], r.bb[first:last, at])
-
-    for k in range(3):
+    for k in range(CHUNKS):
         gather_back(k)
-    early = [combined(0, 192, slice(512 * q, 512 * q + 512)) for q in range(4)]
-    gather_back(3)
-    for q in range(4):
-        at = slice(512 * q, 512 * q + 512)
-        total = r.stream[:, at].astype(F32) + early[q] + combined(192, 256, at)
-        r.out[:, at] = total.astype(BF16)
+        span = slice(64 * k, 64 * k + 64)
+        for q in range(4):
+            at = slice(512 * q, 512 * q + 512)
+            total = r.oacc[:, at] + tn(r.whi[span, :], r.bb[span, at]) + tn(r.wlo[span, :], r.bb[span, at])
+            if k < CHUNKS - 1:
+                r.oacc[:, at] = total
+            else:
+                r.out[:, at] = total.astype(BF16)
 
     for batch in batches:
         batch.wait_send()
-    for o in (1, 2, 3):
-        to_owner(o).wait_send()
+    for cs in range(2):
+        for side in range(2):
+            hop_copy(cs, side).wait_send()
+            for merged in (False, True):
+                owner_copy(cs, side, merged).wait_send()
     for cp in weights:
         cp.wait_send()
-    for src, dst, ssem, rsem in ((r.send, r.recv, r.ssem, r.srecv), (r.ret, r.bk, r.bsend, r.brecv)):
-        remote(src.at[pl.ds(0, 63)], dst.at[pl.ds(0, 63)], ssem.at[0], rsem.at[0], facing).wait_send()
+    for src, dst, ssem, rsem in (
+        (r.send0, r.recv0, r.ssem.at[0], r.srecv.at[0]),
+        (r.send1, r.recv1, r.ssem.at[1], r.srecv.at[4]),
+        (r.ret, r.bk, r.bsend.at[0], r.brecv.at[0]),
+    ):
+        remote(src.at[pl.ds(0, 63)], dst.at[pl.ds(0, 63)], ssem, rsem, facing).wait_send()
     for k in range(CHUNKS):
         forward(k).wait_send()
         partial(k).wait_send()

time: 112 us -> 99.9 us (0.89)
  Pallas kernels: 110 us -> 98 us
    pallas_call x1, Pallas kernels: 110 us -> 98 us  [body(): pl.pallas_call(layer_kernel, name='layer', out_shape=jax.ShapeDtypeStruct...]
where the time goes in v1:
time: 99.9 us; the launch traced here: 99.8 us
  Pallas kernels  98 us (98%)
  local copies, waits for them, and re-layouts  1.77 us (2%)
    pallas_call x1, Pallas kernels, body(): pl.pallas_call(layer_kernel, name='layer', out_shape=jax.ShapeDtypeStruct...  98 us

profile of v1, /device:TPU:1, one launch (start us, length us, event | category | flops | bytes accessed | tf_op | source)
XLA Modules:
  0.0 99.8 jit_solution(5920244981696398710)
XLA Ops:
  0.0 98.0 %layer.1 = bf16[96,2048]{1,0:T(8,128)(2,1)} custom-call(bf16[96,2048]{1,0:T(8,128)(2,1)} %refs_0_.1, bf16[384,128]{1,0:T(8,128)(2,1)} %refs_1_.1, bf16[384,128]{1,0:T(8,128)(2,1)} %refs_2_.1, bf16[384,256]{1,0:T(8,128)(2,1)} %refs_3_.1, bf16[384,256]{1,0:T(8,128)(2,1)} %refs_4_.1, bf16[2,384,128]{2,1,0:T(8,128)(2,1)} %refs_5_.1, f32[1,128]{1,0:T(1,128)} %bitcast.8, ...), custom_call_target="tpu_custom_call" | custom-call | tf_op jit(solution)/shard_map/layer/pallas_call | solution.py:603
  98.0 1.8 %copy.24 = bf16[96,2048]{1,0:T(8,128)(2,1)} copy(bf16[96,2048]{1,0:T(8,128)(2,1)} %layer.1) | data formatting | bytes 786432

commit v2 on v1

--- a/solution.py
+++ b/solution.py
@@ -140,10 +140,15 @@
     for name, pairs in plan.items():
         loads[name] = []
         for src, dst in pairs:
-            cp = pltpu.make_async_copy(src, dst, r.lsem.at[count])
+            loads[name].append(pltpu.make_async_copy(src, dst, r.lsem.at[count]))
             count += 1
-            cp.start()
-            loads[name].append(cp)
+
+    def load(names):
+        for name in names:
+            for cp in loads[name]:
+                cp.start()
+
+    load("dkv")
 
     def loaded(names):
         for name in names:
@@ -198,6 +203,7 @@
                 r.add[way, n, :, 128 * i : 128 * i + 128] = b[:, 128 * way : 128 * way + 128]
 
     loaded("dkv")
+    load("q")
     for n in range(NB):
         keys_of(n)
 
@@ -238,6 +244,8 @@
     for o in (4, 3, 5, 2, 6, 1, 7):
         plane_copy(r.s1, r.r1, 0, o).start()
 
+    load("giosw")
+
     def queries_of(n):
         rows = pl.ds(n * BLOCK, BLOCK)
         q = r.q[rows, :].astype(F32) * scale
@@ -407,12 +415,14 @@
     half = across // 2
     near = 1 - x % 2
     far = 1 - near
-    for i in range(3):
-        read_out(3 * half + i)
+    odd = across % 2
+    read_out(3 * half + odd)
+    read_out(3 * half + odd + 1)
     loaded("o")
     project(across, 3, 0)
     hop_copy(0, 0).start()
     hop_copy(0, 1).start()
+    read_out(3 * half + 2 - 2 * odd)
     for i in range(3):
         read_out(3 * (1 - half) + i)
     to_neighbour(near, 0)
@@ -436,8 +446,8 @@
         for e in range(rows.shape[0] // 4):
             dst[first + e, :, at] = rows[4 * e : 4 * e + 4, :]
 
-    def slabs_out(src, dst, ssem, rsem, k):
-        for i in (2 * k, 2 * k + 1):
+    def slabs_out(src, dst, ssem, rsem, *groups):
+        for i in groups:
             @pl.loop(1 if ORDER[i] == 0 else 0, 8)
             def _(o):
                 t = (p + o) % 8
@@ -461,7 +471,7 @@
             sides[cs][1][8 + p] = sides[cs][0][8 + p]
 
     def dispatch(cs, k):
-        slabs_out(*sides[cs], r.ssem.at[cs], r.srecv.at[4 * cs + k], k)
+        slabs_out(*sides[cs], r.ssem.at[cs], r.srecv.at[4 * cs + k], 2 * k, 2 * k + 1)
 
     own_rows(0)
     fill(0, 0)
@@ -535,14 +545,15 @@
 
     def give_back(k):
         partial(k).wait_recv()
-        span = slice(64 * k, 64 * k + 64)
-        for q in range(4):
-            at = slice(512 * q, 512 * q + 512)
-            rows = r.yown[span, at] + r.yrecv[span, at].astype(F32)
-            scatter_rows(r.ret, 16 * k, rows.astype(BF16), at)
-        if k == 0:
-            r.bk[8 + p] = r.ret[8 + p]
-        slabs_out(r.ret, r.bk, r.bsend.at[0], r.brecv.at[k], k)
+        for i in (2 * k, 2 * k + 1):
+            span = slice(32 * i, 32 * i + 32)
+            for q in range(4):
+                at = slice(512 * q, 512 * q + 512)
+                rows = r.yown[span, at] + r.yrecv[span, at].astype(F32)
+                scatter_rows(r.ret, 8 * i, rows.astype(BF16), at)
+            if ORDER[i] == 0:
+                r.bk[8 * i + p] = r.ret[8 * i + p]
+            slabs_out(r.ret, r.bk, r.bsend.at[0], r.brecv.at[k], i)
 
     arrive(0)
     arrive(1)

time: 99.9 us -> 99.7 us (level)
  no operation moved by 1% of the time
where the time goes in v2:
time: 99.7 us; the launch traced here: 99.6 us
  Pallas kernels  97.8 us (98%)
  local copies, waits for them, and re-layouts  1.77 us (2%)
    pallas_call x1, Pallas kernels, body(): pl.pallas_call(layer_kernel, name='layer', out_shape=jax.ShapeDtypeStruct...  97.8 us

profile of v2, /device:TPU:1, one launch (start us, length us, event | category | flops | bytes accessed | tf_op | source)
XLA Modules:
  0.0 99.6 jit_solution(5853380303820959951)
XLA Ops:
  0.0 97.8 %layer.1 = bf16[96,2048]{1,0:T(8,128)(2,1)} custom-call(bf16[96,2048]{1,0:T(8,128)(2,1)} %refs_0_.1, bf16[384,128]{1,0:T(8,128)(2,1)} %refs_1_.1, bf16[384,128]{1,0:T(8,128)(2,1)} %refs_2_.1, bf16[384,256]{1,0:T(8,128)(2,1)} %refs_3_.1, bf16[384,256]{1,0:T(8,128)(2,1)} %refs_4_.1, bf16[2,384,128]{2,1,0:T(8,128)(2,1)} %refs_5_.1, f32[1,128]{1,0:T(1,128)} %bitcast.8, ...), custom_call_target="tpu_custom_call" | custom-call | tf_op jit(solution)/shard_map/layer/pallas_call | solution.py:614
  97.8 1.8 %copy.24 = bf16[96,2048]{1,0:T(8,128)(2,1)} copy(bf16[96,2048]{1,0:T(8,128)(2,1)} %layer.1) | data formatting | bytes 786432
